TPU v7x, 32 devices: a whole 2x2x4 slice. The times are simulated.
32 devices in a mesh: dp: 4 (over y, x), kv: 4 (over z), tp: 2 (over core).
Axes of the slice: x: 2, y: 2, z: 4, core: 2. Of those that a mesh axis runs over, the one named last changes fastest.
Arguments:
- tokens: bfloat16 [32, 2048], P('dp', ('kv', 'tp')), may hold values from -6 to 6
- gate_first: bfloat16 [2048, 5632], P(None, ('kv', 'tp')), may hold values from -0.110485435 to 0.110485435
- up_first: bfloat16 [2048, 5632], P(None, ('kv', 'tp')), may hold values from -0.110485435 to 0.110485435
- down_first: bfloat16 [5632, 2048], P(('kv', 'tp')), may hold values from -0.13325045 to 0.13325045
- gate_second: bfloat16 [2048, 5632], P(None, ('kv', 'tp')), may hold values from -0.110485435 to 0.110485435
- up_second: bfloat16 [2048, 5632], P(None, ('kv', 'tp')), may hold values from -0.110485435 to 0.110485435
- down_second: bfloat16 [5632, 2048], P(('kv', 'tp')), may hold values from -0.13325045 to 0.13325045
- query_weight: bfloat16 [2048, 1024], P('kv', 'tp'), may hold values from -0.125 to 0.125
- key_weight: bfloat16 [2048, 1024], P('kv', 'tp'), may hold values from -0.125 to 0.125
- value_weight: bfloat16 [2048, 1024], P('kv', 'tp'), may hold values from -0.125 to 0.125
- outgate_weight: bfloat16 [2048, 1024], P('kv', 'tp'), may hold values from -0.125 to 0.125
- decay_weight: bfloat16 [2048, 8], replicated, may hold values from -0.25 to 0.25
- write_weight: bfloat16 [2048, 8], replicated, may hold values from -0.25 to 0.25
- decay_rate: float32 [8], P('tp'), may hold values from -3 to 1
- norm_gain: float32 [128], replicated, may hold values from 0.1 to 1.9
- layer_gain: float32 [3, 2048], replicated, may hold values from 0.1 to 1.9
- out_weight: bfloat16 [1024, 2048], P('tp', 'kv'), may hold values from -0.375 to 0.375
- state: float32 [32, 8, 128, 128], P(('dp', 'kv'), 'tp'), may hold values from -0.6 to 0.6
Outputs:
- layer_out: bfloat16 [32, 2048], P('dp', ('kv', 'tp'))
- new_state: float32 [32, 8, 128, 128], P(('dp', 'kv'), 'tp')
All inputs are finite; a program needn't handle non-finite values.
Results may differ from a plain program's by a relative error of at most 0.015.
Values may be sent and summed in bfloat16 or wider, within the bound.
A program may use at most 64 MiB of HBM per device.

v0:
```python
import jax
import jax.numpy as jnp
from jax import lax
from jax.sharding import PartitionSpec as P

residual_scale = 2.0**0.25
ln_eps = 1e-05
rms_eps = 1e-06


def finish_norm(values, total, squares, width, gain):
    mean = total[:, None] / width
    spread = squares[:, None] / width - mean * mean
    return ((values - mean) * lax.rsqrt(spread + ln_eps) * gain).astype(jnp.bfloat16)


def spread_norm(rows, gain, width):
    values = rows.astype(jnp.float32)
    total, squares = lax.psum((jnp.sum(values, -1), jnp.sum(values * values, -1)), ("kv", "tp"))
    return finish_norm(values, total, squares, width, gain)


def whole_norm(rows, gain):
    values = rows.astype(jnp.float32)
    return finish_norm(
        values, jnp.sum(values, -1), jnp.sum(values * values, -1), values.shape[1], gain
    )


def unit_rows(values):
    return values * lax.rsqrt(jnp.sum(values * values, -1, keepdims=True) + rms_eps)


def shards(
    tokens,
    gate_first,
    up_first,
    down_first,
    gate_second,
    up_second,
    down_second,
    query_weight,
    key_weight,
    value_weight,
    outgate_weight,
    decay_weight,
    write_weight,
    decay_rate,
    norm_gain,
    layer_gain,
    out_weight,
    state,
):
    kv_index = lax.axis_index("kv")
    tp_index = lax.axis_index("tp")
    width = decay_weight.shape[0]
    own = tokens.shape[1]
    block = query_weight.shape[0]
    local_heads = decay_rate.shape[0]
    key_size = state.shape[2]
    value_size = state.shape[3]
    seq_local = state.shape[0]
    own_start = (kv_index * lax.axis_size("tp") + tp_index) * own
    block_start = kv_index * block
    fold_piece = lax.all_gather(tokens, ("kv", "tp"), axis=1, tiled=True)
    gate = jnp.dot(fold_piece, gate_first, preferred_element_type=jnp.float32)
    up = jnp.dot(fold_piece, up_first, preferred_element_type=jnp.float32)
    hidden = (jax.nn.silu(gate) * up).astype(jnp.bfloat16)
    terms = jnp.dot(hidden, down_first, preferred_element_type=jnp.float32)
    branch = lax.psum_scatter(terms, ("kv", "tp"), scatter_dimension=1, tiled=True)
    first = (residual_scale * tokens.astype(jnp.float32) + 0.5 * branch).astype(jnp.bfloat16)
    first = lax.optimization_barrier(first)
    first_rows = lax.all_gather(first, ("kv", "tp"), axis=1, tiled=True)
    mixed_rows = whole_norm(first_rows, layer_gain[0])
    mixed_own = lax.dynamic_slice_in_dim(mixed_rows, own_start, own, 1)
    mixed_block = lax.dynamic_slice_in_dim(mixed_rows, block_start, block, 1)
    decay_part = lax.dynamic_slice(
        decay_weight, (block_start, tp_index * local_heads), (block, local_heads)
    )
    write_part = lax.dynamic_slice(
        write_weight, (block_start, tp_index * local_heads), (block, local_heads)
    )
    partials = tuple(
        (
            jnp.dot(mixed_block, weight, preferred_element_type=jnp.float32)
            for weight in (
                query_weight,
                key_weight,
                value_weight,
                outgate_weight,
                decay_part,
                write_part,
            )
        )
    )
    summed = lax.psum_scatter(partials, "kv", scatter_dimension=0, tiled=True)
    query_p, key_p, value_p, outgate_p, decay_p, write_p = tuple(
        (piece.astype(jnp.bfloat16).astype(jnp.float32) for piece in summed)
    )
    query = unit_rows(
        jax.nn.silu(query_p).reshape(seq_local, local_heads, key_size)
    ) * key_size ** (-0.5)
    keys = unit_rows(jax.nn.silu(key_p).reshape(seq_local, local_heads, key_size))
    vals = jax.nn.silu(value_p).reshape(seq_local, local_heads, value_size)
    outgate = outgate_p.reshape(seq_local, local_heads, value_size)
    beta = jax.nn.sigmoid(write_p)
    decay = -jnp.exp(decay_rate)[None, :] * jax.nn.softplus(decay_p)
    kept = state * jnp.exp(decay)[..., None, None]
    seen = jnp.einsum("bhk,bhkv->bhv", keys, kept, precision=lax.Precision.HIGHEST)
    delta = beta[..., None] * (vals - seen)
    new_state = kept + keys[..., :, None] * delta[..., None, :]
    outs = jnp.einsum("bhk,bhkv->bhv", query, new_state, precision=lax.Precision.HIGHEST)
    normed = outs * lax.rsqrt(jnp.mean(outs * outs, -1, keepdims=True) + rms_eps) * norm_gain
    heads_out = (
        (normed * jax.nn.silu(outgate))
        .astype(jnp.bfloat16)
        .reshape(seq_local, local_heads * value_size)
    )
    out_terms = jnp.dot(
        lax.all_gather(heads_out, "kv", axis=0, tiled=True),
        out_weight,
        preferred_element_type=jnp.float32,
    )
    mix = lax.psum_scatter(out_terms.astype(jnp.bfloat16), "tp", scatter_dimension=1, tiled=True)
    second = (residual_scale * mixed_own.astype(jnp.float32) + mix.astype(jnp.float32)).astype(
        jnp.bfloat16
    )
    second = lax.optimization_barrier(second)
    second_rows = lax.all_gather(second, ("kv", "tp"), axis=1, tiled=True)
    mlp_rows = whole_norm(second_rows, layer_gain[1])
    mlp_own = lax.dynamic_slice_in_dim(mlp_rows, own_start, own, 1)
    gate_two = jnp.dot(mlp_rows, gate_second, preferred_element_type=jnp.float32)
    up_two = jnp.dot(mlp_rows, up_second, preferred_element_type=jnp.float32)
    hidden_two = (jax.nn.silu(gate_two) * up_two).astype(jnp.bfloat16)
    terms_two = jnp.dot(hidden_two, down_second, preferred_element_type=jnp.float32)
    branch_two = lax.psum_scatter(terms_two, ("kv", "tp"), scatter_dimension=1, tiled=True)
    third = (residual_scale * mlp_own.astype(jnp.float32) + 0.5 * branch_two).astype(jnp.bfloat16)
    third = lax.optimization_barrier(third)
    gain_two = lax.dynamic_slice_in_dim(layer_gain[2], own_start, own)
    layer_out = spread_norm(third, gain_two, width)
    return (layer_out, new_state)


def solution(mesh):
    in_specs = (
        P("dp", ("kv", "tp")),
        P(None, ("kv", "tp")),
        P(None, ("kv", "tp")),
        P(("kv", "tp"), None),
        P(None, ("kv", "tp")),
        P(None, ("kv", "tp")),
        P(("kv", "tp"), None),
        P("kv", "tp"),
        P("kv", "tp"),
        P("kv", "tp"),
        P("kv", "tp"),
        P(),
        P(),
        P("tp"),
        P(),
        P(),
        P("tp", "kv"),
        P(("dp", "kv"), "tp", None, None),
    )
    out_specs = (P("dp", ("kv", "tp")), P(("dp", "kv"), "tp", None, None))
    return jax.shard_map(shards, mesh=mesh, in_specs=in_specs, out_specs=out_specs, check_vma=False)
```

profile of v0, /device:TPU:0, one launch (start us, length us, event | category | flops | bytes accessed | tf_op | source)
XLA Modules:
  0.0 202.2 jit_solution(14864948527991169362)
XLA Ops:
  7.2 0.0 reduce-scatter.4.cloned.1.call-start
  7.2 16.1 %all_gather.12 = bf16[8,2048]{1,0:T(8,128)(2,1)S(1)} all-gather(bf16[8,256]{1,0:T(8,128)(2,1)} %param.18), channel_id=1, replica_groups=mesh['dp'=4,'kv'=4,'tp'=2] {'kv','tp'}, dimensions={1}, use_global_device_ids=true | all-gather | bytes 36864 | tf_op jit(solution)/shard_map/all_gather | solution.py:65
  23.3 2.7 %fusion.71 = f32[8,704]{1,0:T(8,128)S(1)} fusion(bf16[8,2048]{1,0:T(8,128)(2,1)S(1)} %all_gather.12, bf16[2048,704]{0,1:T(8,128)(2,1)} %param.19), kind=kOutput, calls=%fused_computation.121 | convolution fusion | flops 23068672 | bytes 2938880 | tf_op jit(solution)/shard_map/dot_general | solution.py:66
  26.0 4.2 %fusion.3 = f32[8,2048]{1,0:T(8,128)} fusion(bf16[704,2048]{1,0:T(8,128)(2,1)S(1)} %copy-done, bf16[8,2048]{1,0:T(8,128)(2,1)S(1)} %all_gather.12, bf16[2048,704]{0,1:T(8,128)(2,1)} %param.20, f32[8,704]{1,0:T(8,128)S(1)} %fusion.71), kind=kOutput, calls=%fused_computation.5 | convolution fusion | flops 46171136 | bytes 5888000 | tf_op jit(solution)/shard_map/dot_general | solution.py:69
  30.2 0.0 reduce-scatter.4.cloned.1.call-update
  30.2 0.0 reduce-scatter.6.cloned.1.call-start
  30.3 0.6 dynamic-slice.1
  31.6 30.3 %reduce-scatter.4.cloned.1.call-done = f32[8,256]{1,0:T(8,128)} async-done(((f32[8,2048]{1,0:T(8,128)}), f32[8,256]{1,0:T(8,128)}) %reduce-scatter.4.cloned.1.call-update) | async-done | bytes 8208 | tf_op jit(solution)/shard_map/reduce_scatter | solution.py:70
  61.8 0.7 add_convert_fusion.2
  62.5 14.1 %all_gather.13 = bf16[8,2048]{1,0:T(8,128)(2,1)S(1)} all-gather(bf16[8,256]{1,0:T(8,128)(2,1)S(1)} %add_convert_fusion.2), channel_id=1, replica_groups=mesh['dp'=4,'kv'=4,'tp'=2] {'kv','tp'}, dimensions={1}, use_global_device_ids=true | all-gather | bytes 36864 | tf_op jit(solution)/shard_map/all_gather | solution.py:73
  76.6 0.2 convert_reduce_fusion.1
  76.8 0.1 fusion.9
  76.9 0.9 fusion.40
  77.8 0.9 fusion.38
  78.6 1.2 fusion.48
  79.9 1.2 fusion.45
  81.1 1.2 fusion.43
  82.3 1.2 fusion.51
  83.5 17.5 %all-reduce.7 = (bf16[8,512]{1,0:T(8,128)(2,1)}, bf16[8,512]{1,0:T(8,128)(2,1)}, bf16[8,512]{1,0:T(8,128)(2,1)S(1)}, bf16[8,512]{1,0:T(8,128)(2,1)S(1)}, bf16[8,4]{1,0:T(8,128)(2,1)}, /*index=5*/bf16[8,4]{1,0:T(8,128)(2,1)}) all-reduce(f32[8,512]{1,0:T(8,128)S(1)} %fusion.43, ...), channel_id=8, replica_groups=mesh['dp'=4,'kv'=4,'tp'=2] {'kv'}, use_global_device_ids=true, to_apply=%region_11.12.clone | all-reduce | flops 16448 | bytes 98688
  101.0 0.7 fusion.53
  101.7 0.7 convert_multiply_fusion.5
  102.5 0.1 multiply_reduce_fusion.2
  102.6 0.1 multiply_multiply_fusion
  102.7 0.1 multiply_reduce_fusion.1
  102.8 0.1 broadcast_multiply_fusion
  102.9 0.7 fusion.59
  103.6 0.6 fusion.4
  104.2 0.1 subtract_multiply_fusion
  104.3 0.2 multiply_add_fusion
  104.5 0.8 copy-done.2
  105.3 0.5 fusion.72
  105.8 0.1 multiply_reduce_fusion
  105.9 0.1 fusion.42
  106.0 11.9 %all-gather = bf16[4,2,512]{2,1,0:T(2,128)(2,1)S(1)} all-gather(bf16[1,2,512]{2,1,0:T(2,128)(2,1)S(1)} %reshape.107), channel_id=1, replica_groups=mesh['dp'=4,'kv'=4,'tp'=2] {'kv'}, dimensions={0}, use_global_device_ids=true | all-gather | bytes 10240 | tf_op jit(solution)/shard_map/all_gather | solution.py:120
  118.0 1.8 convolution_convert_fusion
  119.8 0.0 reduce-scatter.8.cloned.1.call-start
  119.9 6.1 %reduce-scatter.6.cloned.1.call-done = bf16[8,256]{1,0:T(8,128)(2,1)} async-done(((bf16[8,512]{1,0:T(8,128)(2,1)}), bf16[8,256]{1,0:T(8,128)(2,1)}) %reduce-scatter.6.cloned.1.call-update) | async-done | bytes 4112 | tf_op jit(solution)/shard_map/reduce_scatter | solution.py:124
  126.0 0.7 add_convert_fusion.1
  126.7 14.3 %all_gather.15 = bf16[8,2048]{1,0:T(8,128)(2,1)S(1)} all-gather(bf16[8,256]{1,0:T(8,128)(2,1)S(1)} %add_convert_fusion.1), channel_id=1, replica_groups=mesh['dp'=4,'kv'=4,'tp'=2] {'kv','tp'}, dimensions={1}, use_global_device_ids=true | all-gather | bytes 36864 | tf_op jit(solution)/shard_map/all_gather | solution.py:129
  141.0 0.2 convert_reduce_fusion
  141.2 0.1 fusion.13
  141.3 2.7 %fusion.73 = f32[8,704]{1,0:T(8,128)S(1)} fusion(bf16[8,2048]{1,0:T(8,128)(2,1)S(1)} %fusion.13, bf16[2048,704]{0,1:T(8,128)(2,1)} %param.22), kind=kOutput, calls=%fused_computation.123 | convolution fusion | flops 23068672 | bytes 2938880 | tf_op jit(solution)/shard_map/dot_general | solution.py:132
  143.9 5.0 %fusion.2 = f32[8,2048]{1,0:T(8,128)} fusion(bf16[704,2048]{1,0:T(8,128)(2,1)} %param.24, bf16[8,2048]{1,0:T(8,128)(2,1)S(1)} %fusion.13, bf16[2048,704]{0,1:T(8,128)(2,1)} %param.23, f32[8,704]{1,0:T(8,128)S(1)} %fusion.73), kind=kOutput, calls=%fused_computation.4 | convolution fusion | flops 46171136 | bytes 5888000 | tf_op jit(solution)/shard_map/dot_general | solution.py:135
  148.9 31.5 %reduce-scatter.8.cloned.1.call-done = f32[8,256]{1,0:T(8,128)} async-done(((f32[8,2048]{1,0:T(8,128)}), f32[8,256]{1,0:T(8,128)}) %reduce-scatter.8.cloned.1.call-update) | async-done | bytes 8208 | tf_op jit(solution)/shard_map/reduce_scatter | solution.py:136
  180.5 0.7 add_convert_fusion
  181.2 0.1 convert_reduce_fusion.2
  181.3 13.7 %all-reduce.6 = (f32[8]{0:T(128)S(1)}, f32[8]{0:T(128)S(1)}) all-reduce(f32[8]{0:T(128)S(1)} %get-tuple-element.7, f32[8]{0:T(128)S(1)} %get-tuple-element.6), channel_id=1, replica_groups=mesh['dp'=4,'kv'=4,'tp'=2] {'kv','tp'}, use_global_device_ids=true, to_apply=%region_19.20 | all-reduce | flops 16 | bytes 128 | tf_op jit(solution)/shard_map/psum | solution.py:19
  195.0 0.7 fusion.29
  (33 shorter events, 0.3 us)
Async XLA Ops:
  7.2 18.8 %copy-start = (bf16[704,2048]{1,0:T(8,128)(2,1)S(1)}, bf16[704,2048]{1,0:T(8,128)(2,1)}, u32[]{:S(2)}) copy-start(bf16[704,2048]{1,0:T(8,128)(2,1)} %param.21) | copy-start | bytes 8650756
  7.2 54.6 %reduce-scatter.4.cloned.1.call-start = ((), (), s32[]{:S(2)}) async-start(), calls=%async_computation.3 | async-start | bytes 73728 | tf_op jit(solution)/shard_map/reduce_scatter | solution.py:70
  25.9 4.3 %copy-start.3 = (f32[3,2048]{1,0:T(4,128)S(1)}, f32[3,2048]{1,0:T(4,128)}, u32[]{:S(2)}) copy-start(f32[3,2048]{1,0:T(4,128)} %param.33) | copy-start | bytes 73732
  25.9 4.4 %copy-start.7 = (u32[32]{0:T(128)S(1)}, u32[32]{0:T(128)}, u32[]{:S(2)}) copy-start(u32[32]{0:T(128)} %constant.62) | copy-start | bytes 388
  26.0 5.6 %copy-start.6 = (f32[4]{0:T(128)S(1)}, f32[4]{0:T(128)}, u32[]{:S(2)}) copy-start(f32[4]{0:T(128)} %param.31) | copy-start | bytes 52
  26.0 35.9 %copy-start.4 = (bf16[8,256]{1,0:T(8,128)(2,1)S(1)}, bf16[8,256]{1,0:T(8,128)(2,1)}, u32[]{:S(2)}) copy-start(bf16[8,256]{1,0:T(8,128)(2,1)} %param.18) | copy-start | bytes 12292
  26.0 77.6 %copy-start.1 = (f32[2,4,128,128]{3,2,1,0:T(8,128)S(1)}, f32[2,4,128,128]{3,2,1,0:T(8,128)}, u32[]{:S(2)}) copy-start(f32[2,4,128,128]{3,2,1,0:T(8,128)} %param.35) | copy-start | bytes 1572868
  30.2 75.8 %copy-start.5 = (f32[128]{0:T(128)S(1)}, f32[128]{0:T(128)}, u32[]{:S(2)}) copy-start(f32[128]{0:T(128)} %param.32) | copy-start | bytes 1540
  30.2 95.8 %reduce-scatter.6.cloned.1.call-start = ((), (), s32[]{:S(2)}) async-start(), calls=%async_computation.4 | async-start | bytes 12288 | tf_op jit(solution)/shard_map/reduce_scatter | solution.py:124
  104.5 0.8 copy-start.2
  119.8 60.6 %reduce-scatter.8.cloned.1.call-start = ((), (), s32[]{:S(2)}) async-start(), calls=%async_computation.5 | async-start | bytes 73728 | tf_op jit(solution)/shard_map/reduce_scatter | solution.py:136
Sparse Core Ops, SparseCore 0:
  30.3 31.4 reduce-scatter.3
  119.9 6.0 reduce-scatter.5
  149.0 31.3 reduce-scatter.7
where the time goes:
time: 203 us; the launch traced here: 202 us
  blocking collectives  87.5 us (43%)
  waiting for transfers between devices  67.9 us (33%)
  matrix products  24.1 us (12%)
  between operations  14.6 us (7%)
  other arithmetic  6.39 us (3%)
    reduce_scatter x1, waiting for transfers between devices, shards(): lax.psum_scatter(terms_two, ('kv', 'tp'), scatter_dimension=1, tiled=True)  31.5 us
    reduce_scatter x1, waiting for transfers between devices, shards(): lax.psum_scatter(terms, ('kv', 'tp'), scatter_dimension=1, tiled=True)  30.3 us
    unnamed x1, blocking collectives  17.5 us
    all_gather x1, blocking collectives, shards(): fold_piece = lax.all_gather(tokens, ('kv', 'tp'), axis=1, tiled=True)  16.1 us
    all_gather x1, blocking collectives, shards(): second_rows = lax.all_gather(second, ('kv', 'tp'), axis=1, tiled=True)  14.3 us
    all_gather x1, blocking collectives, shards(): first_rows = lax.all_gather(first, ('kv', 'tp'), axis=1, tiled=True)  14.1 us
    psum x1, blocking collectives, spread_norm(): lax.psum((jnp.sum(values, -1), jnp.sum(values * values, -1)), ('kv', 'tp'))  13.7 us
    all_gather x1, blocking collectives, shards(): lax.all_gather(heads_out, 'kv', axis=0, tiled=True)  11.9 us
  transfers between devices with their start and end apart: 3, of which 3 were waited for; matrix products, arithmetic and copies ran while one was open for 0% of the time, Pallas kernels for 0%

commit v1 on v0

--- a/solution.py
+++ b/solution.py
@@ -1,11 +1,19 @@
+import functools
+
 import jax
 import jax.numpy as jnp
 from jax import lax
+from jax.experimental import pallas as pl
+from jax.experimental.pallas import tpu as pltpu
 from jax.sharding import PartitionSpec as P
 
 residual_scale = 2.0**0.25
 ln_eps = 1e-05
 rms_eps = 1e-06
+f32 = jnp.float32
+bf16 = jnp.bfloat16
+
+TOK, RED1, GAINS, PAIR, STAT, PROJ, HEADS, MIX, ROWS2, RED2, STAT2 = range(11)
 
 
 def finish_norm(values, total, squares, width, gain):
@@ -31,7 +39,7 @@
     return values * lax.rsqrt(jnp.sum(values * values, -1, keepdims=True) + rms_eps)
 
 
-def shards(
+def shards_by_collectives(
     tokens,
     gate_first,
     up_first,
@@ -141,6 +149,456 @@
     return (layer_out, new_state)
 
 
+def dot(a, b):
+    return jnp.dot(a, b, preferred_element_type=f32)
+
+
+def silu(x):
+    return x * jax.nn.sigmoid(x)
+
+
+def kernel(
+    n_kv,
+    n_tp,
+    tokens,
+    gate_first,
+    up_first,
+    down_first,
+    gate_second,
+    up_second,
+    down_second,
+    query_weight,
+    key_weight,
+    value_weight,
+    outgate_weight,
+    decay_weight,
+    write_weight,
+    decay_rate,
+    norm_gain,
+    layer_gain,
+    out_weight,
+    state,
+    layer_out,
+    new_state,
+    tok,
+    g1,
+    u1,
+    d1,
+    g2,
+    u2,
+    d2,
+    wq,
+    wk,
+    wv,
+    wo,
+    wd,
+    ww,
+    rate,
+    ngain,
+    lgain,
+    ow,
+    st,
+    ns,
+    out_v,
+    red_out,
+    red_in,
+    red_out2,
+    red_in2,
+    gain_buf,
+    pair_buf,
+    stat_buf,
+    proj_out,
+    proj_in,
+    head_buf,
+    mix_out,
+    mix_in,
+    rows_buf,
+    stat2_buf,
+    stat_rows,
+    load_sem,
+    send_sem,
+    recv_sem,
+):
+    n = n_kv * n_tp
+    kv = lax.axis_index("kv")
+    tp = lax.axis_index("tp")
+    me = kv * n_tp + tp
+    group, own = tokens.shape
+    width = n * own
+    block = wq.shape[0]
+    seqs, heads, dk, dv = state.shape
+    pairs = seqs * heads
+    cols = heads * dk
+    own_start = pl.multiple_of(me * own, own)
+    block_start = pl.multiple_of(kv * block, block)
+
+    loads = {}
+
+    def load(name, src, dst):
+        loads[name] = pltpu.make_async_copy(src, dst, load_sem.at[len(loads)])
+        loads[name].start()
+
+    load("tok", tokens, tok.at[me])
+    load("g1", gate_first, g1)
+    load("u1", up_first, u1)
+    load("d1", down_first, d1)
+    load("lgain", layer_gain, lgain)
+    load("wq", query_weight, wq)
+    load("wk", key_weight, wk)
+    load("wv", value_weight, wv)
+    load("wo", outgate_weight, wo)
+    load("wd", decay_weight.at[pl.ds(block_start, block)], wd)
+    load("ww", write_weight.at[pl.ds(block_start, block)], ww)
+    load("rate", decay_rate, rate)
+    load("ngain", norm_gain, ngain)
+    load("st", state, st)
+    load("ow", out_weight, ow)
+    load("g2", gate_second, g2)
+    load("u2", up_second, u2)
+    load("d2", down_second, d2)
+
+    def peer_of(step):
+        other = lax.rem(me + step, n)
+        return other, lax.div(other, n_tp), lax.rem(other, n_tp)
+
+    barrier = pltpu.get_barrier_semaphore()
+    for step in range(1, n):
+        _, pk, pt = peer_of(step)
+        pl.semaphore_signal(
+            barrier,
+            inc=1,
+            device_id={"kv": pk, "tp": pt},
+            device_id_type=pl.DeviceIdType.MESH,
+        )
+    pl.semaphore_wait(barrier, n - 1)
+
+    sends = []
+
+    def send(kind, src, dst, pk, pt):
+        other = pk * n_tp + pt
+        copy = pltpu.make_async_remote_copy(
+            src_ref=src,
+            dst_ref=dst,
+            send_sem=send_sem.at[kind, other],
+            recv_sem=recv_sem.at[kind, me],
+            device_id={"kv": pk, "tp": pt},
+            device_id_type=pl.DeviceIdType.MESH,
+        )
+        copy.start()
+        sends.append(copy)
+
+    def receive(kind, dst, pk, pt):
+        other = pk * n_tp + pt
+        pltpu.make_async_remote_copy(
+            src_ref=dst,
+            dst_ref=dst,
+            send_sem=send_sem.at[kind, other],
+            recv_sem=recv_sem.at[kind, other],
+            device_id={"kv": pk, "tp": pt},
+            device_id_type=pl.DeviceIdType.MESH,
+        ).wait_recv()
+
+    def send_all(kind, src_of, dst):
+        for step in range(1, n):
+            other, pk, pt = peer_of(step)
+            send(kind, src_of(other), dst, pk, pt)
+
+    def receive_all(kind, buf):
+        for step in range(1, n):
+            other, pk, pt = peer_of(step)
+            receive(kind, buf.at[other], pk, pt)
+
+    def send_kv(kind, src_of, dst):
+        for step in range(1, n_kv):
+            pk = lax.rem(kv + step, n_kv)
+            send(kind, src_of(pk), dst, pk, tp)
+
+    def receive_kv(kind, buf):
+        for step in range(1, n_kv):
+            pk = lax.rem(kv + step, n_kv)
+            receive(kind, buf.at[pk], pk, tp)
+
+    other_tp = lax.rem(tp + 1, n_tp)
+
+    loads["tok"].wait()
+    send_all(TOK, lambda other: tok.at[me], tok.at[me])
+    loads["g1"].wait()
+    loads["u1"].wait()
+    receive_all(TOK, tok)
+
+    def feed_forward(rows, gw, uw, dw, wait_down, send_buf):
+        x = jnp.concatenate(rows, axis=1)
+        hidden = (silu(dot(x, gw[...])) * dot(x, uw[...])).astype(bf16)
+        wait_down()
+        terms = dot(hidden, dw[...]).astype(bf16)
+        for part in range(n):
+            send_buf[part] = terms[:, part * own : (part + 1) * own]
+
+    feed_forward([tok[s] for s in range(n)], g1, u1, d1, loads["d1"].wait, red_out)
+    send_all(RED1, lambda other: red_out.at[other], red_in.at[me])
+    red_in[me] = red_out[me]
+
+    for name in ("lgain", "wq", "wk", "wv", "wo", "wd", "ww"):
+        loads[name].wait()
+    gain_block = lgain[0:1, pl.ds(block_start, block)]
+
+    def project(x):
+        parts = [dot(x, w[...]) for w in (wq, wk, wv, wo)]
+        for w in (wd, ww):
+            parts.append(dot(x, w[...]))
+        return parts
+
+    n_small = wd.shape[1]
+    spans = [i * cols for i in range(4)] + [4 * cols, 4 * cols + 128]
+    lengths = [cols] * 4 + [n_small] * 2
+    gains = project(jnp.broadcast_to(gain_block, (group, block)).astype(bf16))
+    gain_buf[kv] = jnp.zeros(gain_buf.shape[1:], f32)
+    for part, start, length in zip(gains, spans, lengths):
+        gain_buf[kv, :, start : start + length] = part[0:1]
+    send_kv(GAINS, lambda pk: gain_buf.at[kv], gain_buf.at[kv])
+
+    receive_all(RED1, red_in)
+    branch = red_in[0].astype(f32)
+    for s in range(1, n):
+        branch = branch + red_in[s].astype(f32)
+    first = (residual_scale * tok[me].astype(f32) + 0.5 * branch).astype(bf16)
+    pair_buf[tp] = first
+    send(PAIR, pair_buf.at[tp], pair_buf.at[tp], kv, other_tp)
+    first = first.astype(f32)
+
+    def sums(values):
+        lane = lax.broadcasted_iota(jnp.int32, (group, 128), 1)
+        total = jnp.sum(values, -1, keepdims=True)
+        squares = jnp.sum(values * values, -1, keepdims=True)
+        return jnp.where(lane == 0, total, jnp.where(lane == 1, squares, 0.0))
+
+    stat_buf[me] = sums(first)
+    send_all(STAT, lambda other: stat_buf.at[me], stat_buf.at[me])
+    receive(PAIR, pair_buf.at[other_tp], kv, other_tp)
+    rows = jnp.concatenate([pair_buf[t].astype(f32) for t in range(n_tp)], axis=1)
+    centre = jnp.sum(rows, -1, keepdims=True) / block
+    partial = project(((rows - centre) * gain_block).astype(bf16))
+    for j in range(n_kv):
+        proj_out[j] = jnp.zeros(proj_out.shape[1:], bf16)
+        for part, start, length in zip(partial, spans, lengths):
+            proj_out[j, :, start : start + length] = part[
+                j * seqs : (j + 1) * seqs
+            ].astype(bf16)
+    send_kv(PROJ, lambda pk: proj_out.at[pk], proj_in.at[kv])
+    proj_in[kv] = proj_out[kv]
+
+    receive_all(STAT, stat_buf)
+    receive_kv(GAINS, gain_buf)
+
+    def moments(buf):
+        total = buf[0]
+        for s in range(1, n):
+            total = total + buf[s]
+        mean = total[:, 0:1] / width
+        spread = total[:, 1:2] / width - mean * mean
+        return mean, lax.rsqrt(spread + ln_eps)
+
+    mean, rstd = moments(stat_buf)
+    own_gain = lgain[0:1, pl.ds(own_start, own)]
+    mixed_own = ((first - mean) * rstd * own_gain).astype(bf16).astype(f32)
+    lane = lax.broadcasted_iota(jnp.int32, (group, 128), 1)
+    packed = jnp.where(lane == n_kv, rstd, 0.0)
+    for j in range(n_kv):
+        local = stat_buf[j * n_tp]
+        for t in range(1, n_tp):
+            local = local + stat_buf[j * n_tp + t]
+        packed = jnp.where(lane == j, local[:, 0:1] / block - mean, packed)
+    stat_rows[...] = packed
+    mine = stat_rows[pl.ds(kv * seqs, seqs), :]
+
+    receive_kv(PROJ, proj_in)
+    summed = jnp.zeros((seqs, proj_in.shape[2]), f32)
+    for j in range(n_kv):
+        summed = summed + proj_in[j].astype(f32) + mine[:, j : j + 1] * gain_buf[j]
+    summed = (summed * mine[:, n_kv : n_kv + 1]).astype(bf16).astype(f32)
+
+    def by_head(base):
+        return jnp.concatenate(
+            [
+                summed[s : s + 1, base + h * dk : base + (h + 1) * dk]
+                for s in range(seqs)
+                for h in range(heads)
+            ],
+            axis=0,
+        )
+
+    def unit(values):
+        return values * lax.rsqrt(jnp.sum(values * values, -1, keepdims=True) + rms_eps)
+
+    query = unit(silu(by_head(0))) * dk ** (-0.5)
+    keys = unit(silu(by_head(cols)))
+    vals = silu(by_head(2 * cols))
+    outgate = by_head(3 * cols)
+    pair_lane = lax.broadcasted_iota(jnp.int32, (pairs, 128), 1)
+    pair_head = lax.rem(lax.broadcasted_iota(jnp.int32, (pairs, 128), 0), heads)
+
+    def per_head(base):
+        spread = jnp.concatenate(
+            [
+                jnp.broadcast_to(summed[s : s + 1, base : base + 128], (heads, 128))
+                for s in range(seqs)
+            ],
+            axis=0,
+        )
+        picked = jnp.where(pair_lane == pair_head + tp * heads, spread, 0.0)
+        return jnp.sum(picked, -1, keepdims=True)
+
+    decay_pre = per_head(4 * cols)
+    beta = jax.nn.sigmoid(per_head(4 * cols + 128))
+    loads["rate"].wait()
+    rate_lane = lax.broadcasted_iota(jnp.int32, (pairs, heads), 1)
+    rate_head = lax.rem(lax.broadcasted_iota(jnp.int32, (pairs, heads), 0), heads)
+    rates = jnp.sum(
+        jnp.where(rate_lane == rate_head, jnp.broadcast_to(rate[...], (pairs, heads)), 0.0),
+        -1,
+        keepdims=True,
+    )
+    softplus = jnp.maximum(decay_pre, 0.0) + jnp.log1p(jnp.exp(-jnp.abs(decay_pre)))
+    factor = jnp.broadcast_to(jnp.exp(-jnp.exp(rates) * softplus), (pairs, dv))
+    beta = jnp.broadcast_to(beta, (pairs, dv))
+    keys_t = jnp.transpose(keys)
+    query_t = jnp.transpose(query)
+    loads["st"].wait()
+    outs = []
+    for s in range(seqs):
+        for h in range(heads):
+            i = s * heads + h
+            kept = st[s, h] * factor[i : i + 1]
+            key = keys_t[:, i : i + 1]
+            seen = jnp.sum(kept * key, 0, keepdims=True)
+            fresh = kept + key * (beta[i : i + 1] * (vals[i : i + 1] - seen))
+            ns[s, h] = fresh
+            outs.append(jnp.sum(fresh * query_t[:, i : i + 1], 0, keepdims=True))
+    outs = jnp.concatenate(outs, axis=0)
+    loads["ngain"].wait()
+    normed = outs * lax.rsqrt(jnp.mean(outs * outs, -1, keepdims=True) + rms_eps) * ngain[...]
+    gated = (normed * silu(outgate)).astype(bf16)
+    for s in range(seqs):
+        for h in range(heads):
+            i = s * heads + h
+            head_buf[kv, s : s + 1, h * dv : (h + 1) * dv] = gated[i : i + 1]
+    send_kv(HEADS, lambda pk: head_buf.at[kv], head_buf.at[kv])
+    store = pltpu.make_async_copy(ns, new_state, load_sem.at[len(loads)])
+    store.start()
+    loads["ow"].wait()
+    receive_kv(HEADS, head_buf)
+    everyone = jnp.concatenate([head_buf[j].astype(f32) for j in range(n_kv)], axis=0)
+    terms = dot(everyone.astype(bf16), ow[...]).astype(bf16)
+    for t in range(n_tp):
+        mix_out[t] = terms[:, t * own : (t + 1) * own]
+    send(MIX, mix_out.at[other_tp], mix_in, kv, other_tp)
+    kept_half = mix_out[tp].astype(f32)
+    receive(MIX, mix_in, kv, other_tp)
+    mix = (kept_half + mix_in[...].astype(f32)).astype(bf16).astype(f32)
+    rows_buf[me] = (residual_scale * mixed_own + mix).astype(bf16)
+    send_all(ROWS2, lambda other: rows_buf.at[me], rows_buf.at[me])
+    loads["g2"].wait()
+    loads["u2"].wait()
+    receive_all(ROWS2, rows_buf)
+
+    second = [rows_buf[s].astype(f32) for s in range(n)]
+    total = sum(jnp.sum(v, -1, keepdims=True) for v in second)
+    squares = sum(jnp.sum(v * v, -1, keepdims=True) for v in second)
+    mean = total / width
+    rstd = lax.rsqrt(squares / width - mean * mean + ln_eps)
+
+    def normalise(v, start):
+        return ((v - mean) * rstd * lgain[1:2, pl.ds(start, own)]).astype(bf16)
+
+    mlp_own = normalise(rows_buf[me].astype(f32), own_start).astype(f32)
+    feed_forward(
+        [normalise(v, s * own) for s, v in enumerate(second)],
+        g2,
+        u2,
+        d2,
+        loads["d2"].wait,
+        red_out2,
+    )
+    send_all(RED2, lambda other: red_out2.at[other], red_in2.at[me])
+    red_in2[me] = red_out2[me]
+    receive_all(RED2, red_in2)
+    branch = red_in2[0].astype(f32)
+    for s in range(1, n):
+        branch = branch + red_in2[s].astype(f32)
+    third = (residual_scale * mlp_own + 0.5 * branch).astype(bf16).astype(f32)
+    stat2_buf[me] = sums(third)
+    send_all(STAT2, lambda other: stat2_buf.at[me], stat2_buf.at[me])
+    receive_all(STAT2, stat2_buf)
+    mean, rstd = moments(stat2_buf)
+    out_v[...] = ((third - mean) * rstd * lgain[2:3, pl.ds(own_start, own)]).astype(bf16)
+    final = pltpu.make_async_copy(out_v, layer_out, load_sem.at[len(loads) + 1])
+    final.start()
+    for copy in sends:
+        copy.wait_send()
+    store.wait()
+    final.wait()
+
+
+def shards(n_kv, n_tp, *args):
+    if args[0].shape[1] % 128 or args[17].shape[2] != 128:
+        return shards_by_collectives(*args)
+    args = list(args)
+    args[13] = args[13].reshape(1, -1)
+    args[14] = args[14].reshape(1, -1)
+    tokens, decay_weight, state = args[0], args[11], args[17]
+    query_weight = args[7]
+    n = n_kv * n_tp
+    group, own = tokens.shape
+    seqs = state.shape[0]
+    block, cols = query_weight.shape
+    small = decay_weight.shape[1]
+    flat = 4 * cols + 2 * 128
+
+    def like(x):
+        return pltpu.VMEM(x.shape, x.dtype)
+
+    scratch = [
+        pltpu.VMEM((n, group, own), bf16),
+        *[like(x) for x in args[1:11]],
+        pltpu.VMEM((block, small), bf16),
+        pltpu.VMEM((block, small), bf16),
+        *[like(x) for x in args[13:18]],
+        like(state),
+        like(tokens),
+        pltpu.VMEM((n, group, own), bf16),
+        pltpu.VMEM((n, group, own), bf16),
+        pltpu.VMEM((n, group, own), bf16),
+        pltpu.VMEM((n, group, own), bf16),
+        pltpu.VMEM((n_kv, 1, flat), f32),
+        pltpu.VMEM((n_tp, group, own), bf16),
+        pltpu.VMEM((n, group, 128), f32),
+        pltpu.VMEM((n_kv, seqs, flat), bf16),
+        pltpu.VMEM((n_kv, seqs, flat), bf16),
+        pltpu.VMEM((n_kv, seqs, cols), bf16),
+        pltpu.VMEM((n_tp, group, own), bf16),
+        pltpu.VMEM((group, own), bf16),
+        pltpu.VMEM((n, group, own), bf16),
+        pltpu.VMEM((n, group, 128), f32),
+        pltpu.VMEM((group, 128), f32),
+        pltpu.SemaphoreType.DMA((20,)),
+        pltpu.SemaphoreType.DMA((11, n)),
+        pltpu.SemaphoreType.DMA((11, n)),
+    ]
+    return pl.pallas_call(
+        functools.partial(kernel, n_kv, n_tp),
+        out_shape=(
+            jax.ShapeDtypeStruct(tokens.shape, tokens.dtype),
+            jax.ShapeDtypeStruct(state.shape, state.dtype),
+        ),
+        in_specs=[pl.BlockSpec(memory_space=pl.ANY)] * len(args),
+        out_specs=(pl.BlockSpec(memory_space=pl.ANY),) * 2,
+        scratch_shapes=scratch,
+        compiler_params=pltpu.CompilerParams(
+            collective_id=0, has_side_effects=True, vmem_limit_bytes=60 * 1024 * 1024
+        ),
+    )(*args)
+
+
 def solution(mesh):
     in_specs = (
         P("dp", ("kv", "tp")),
@@ -163,4 +621,5 @@
         P(("dp", "kv"), "tp", None, None),
     )
     out_specs = (P("dp", ("kv", "tp")), P(("dp", "kv"), "tp", None, None))
-    return jax.shard_map(shards, mesh=mesh, in_specs=in_specs, out_specs=out_specs, check_vma=False)
+    body = functools.partial(shards, mesh.shape["kv"], mesh.shape["tp"])
+    return jax.shard_map(body, mesh=mesh, in_specs=in_specs, out_specs=out_specs, check_vma=False)

time: 203 us -> 60.5 us (0.30)
  blocking collectives: 87.5 us -> 0 us
  waiting for transfers between devices: 67.9 us -> 0 us
  Pallas kernels: 0 us -> 37.5 us
  matrix products: 24.1 us -> 0 us
  local copies, waits for them, and re-layouts: 1.53 us -> 21.9 us
  between operations: 14.6 us -> 0.64 us
  other arithmetic: 6.39 us -> 0 us
    reduce_scatter x3 -> x0, waiting for transfers between devices: 67.9 us -> none  [the longest x1 31.5 us: shards(): lax.psum_scatter(terms_two, ('kv', 'tp'), scatter_dimension=1, tiled=True)]
    all_gather x4 -> x0, blocking collectives: 56.4 us -> none  [the longest x1 16.1 us: shards(): fold_piece = lax.all_gather(tokens, ('kv', 'tp'), axis=1, tiled=True)]
    pallas_call x0 -> x1, Pallas kernels: none -> 37.5 us  [shards(): pl.pallas_call(functools.partial(kernel, n_kv, n_tp), out_shape=(jax.Shap...]
    dot_general x13 -> x0, matrix products: 24.1 us -> none  [the longest x6 6.67 us: shards(): jnp.dot(mixed_block, weight, preferred_element_type=jnp.float32)]
    unnamed x19 -> x12, local copies, waits for them, and re-layouts: 1.44 us -> 21.9 us
    unnamed x1 -> x0, blocking collectives: 17.5 us -> none
    psum x1 -> x0, blocking collectives: 13.7 us -> none  [spread_norm(): lax.psum((jnp.sum(values, -1), jnp.sum(values * values, -1)), ('kv', 'tp'))]
    convert_element_type x7 -> x0, other arithmetic: 3.01 us -> none  [the longest x3 0.85 us: finish_norm(): ((values - mean) * lax.rsqrt(spread + ln_eps) * gain).astype(jnp.bfloat16)]
  transfers between devices with their start and end apart: 3 -> 0, of which waited for: 3 -> 0; matrix products, arithmetic and copies ran while one was open for 0% -> 0% of each run, Pallas kernels for 0% -> 0%
where the time goes in v1:
time: 60.5 us; the launch traced here: 60.1 us
  Pallas kernels  37.5 us (62%)
  local copies, waits for them, and re-layouts  21.9 us (36%)
  between operations  0.64 us (1%)
    pallas_call x1, Pallas kernels, shards(): pl.pallas_call(functools.partial(kernel, n_kv, n_tp), out_shape=(jax.Shap...  37.5 us
    unnamed x12, local copies, waits for them, and re-layouts  21.9 us

profile of v1, /device:TPU:0, one launch (start us, length us, event | category | flops | bytes accessed | tf_op | source)
XLA Modules:
  0.0 60.1 jit_solution(4998801115024732591)
XLA Ops:
  0.6 1.8 %copy.24.decay_weight = bf16[2048,8]{1,0:T(8,128)(2,1)} copy(bf16[2048,8]{0,1:T(8,128)(2,1)} %param.29) | data formatting | bytes 65536 | tf_op args[11]
  2.4 1.8 %copy.25.write_weight = bf16[2048,8]{1,0:T(8,128)(2,1)} copy(bf16[2048,8]{0,1:T(8,128)(2,1)} %param.30) | data formatting | bytes 65536 | tf_op args[12]
  4.2 0.0 copy-start
  4.2 4.8 %copy.20.gate_first = bf16[2048,704]{1,0:T(8,128)(2,1)} copy(bf16[2048,704]{0,1:T(8,128)(2,1)} %param.19) | data formatting | bytes 5767168 | tf_op args[1]
  8.9 0.0 copy-done
  8.9 2.8 %copy.21.up_first = bf16[2048,704]{1,0:T(8,128)(2,1)} copy(bf16[2048,704]{0,1:T(8,128)(2,1)S(1)} %copy-done) | data formatting | bytes 5767168 | tf_op args[2]
  11.8 0.0 copy-start.1
  11.8 4.8 %copy.22.gate_second = bf16[2048,704]{1,0:T(8,128)(2,1)} copy(bf16[2048,704]{0,1:T(8,128)(2,1)} %param.22) | data formatting | bytes 5767168 | tf_op args[4]
  16.6 0.0 copy-done.1
  16.6 2.8 %copy.23.up_second = bf16[2048,704]{1,0:T(8,128)(2,1)} copy(bf16[2048,704]{0,1:T(8,128)(2,1)S(1)} %copy-done.1) | data formatting | bytes 5767168 | tf_op args[5]
  19.4 37.5 %shard_map.185 = (bf16[8,256]{1,0:T(8,128)(2,1)}, f32[2,4,128,128]{3,2,1,0:T(8,128)}) custom-call(bf16[8,256]{1,0:T(8,128)(2,1)} %tokens.1, bf16[2048,704]{1,0:T(8,128)(2,1)} %copy.20.gate_first, bf16[2048,704]{1,0:T(8,128)(2,1)} %copy.21.up_first, bf16[704,2048]{1,0:T(8,128)(2,1)} %down_first.1, bf16[2048,704]{1,0:T(8,128)(2,1)} %copy.22.gate_second, ...), custom_call_target="tpu_custom_call" | custom-call | tf_op jit(solution)/shard_map/pallas_call | solution.py:587
  56.9 1.3 %copy.28 = bf16[8,256]{1,0:T(8,128)(2,1)} copy(bf16[8,256]{1,0:T(8,128)(2,1)} %get-tuple-element.4) | data formatting | bytes 8192
  58.2 1.9 %copy.29 = f32[2,4,128,128]{3,2,1,0:T(8,128)} copy(f32[2,4,128,128]{3,2,1,0:T(8,128)} %get-tuple-element.5) | data formatting | bytes 1048576
Async XLA Ops:
  4.2 4.8 %copy-start = (bf16[2048,704]{0,1:T(8,128)(2,1)S(1)}, bf16[2048,704]{0,1:T(8,128)(2,1)}, u32[]{:S(2)}) copy-start(bf16[2048,704]{0,1:T(8,128)(2,1)} %param.20) | copy-start | bytes 8650756
  11.8 4.8 %copy-start.1 = (bf16[2048,704]{0,1:T(8,128)(2,1)S(1)}, bf16[2048,704]{0,1:T(8,128)(2,1)}, u32[]{:S(2)}) copy-start(bf16[2048,704]{0,1:T(8,128)(2,1)} %param.23) | copy-start | bytes 8650756

commit v2 on v1

--- a/solution.py
+++ b/solution.py
@@ -151,6 +151,10 @@
 
 def dot(a, b):
     return jnp.dot(a, b, preferred_element_type=f32)
+
+
+def dot_t(a, b):
+    return lax.dot_general(a, b, (((1,), (1,)), ((), ())), preferred_element_type=f32)
 
 
 def silu(x):
@@ -247,8 +251,8 @@
     load("wk", key_weight, wk)
     load("wv", value_weight, wv)
     load("wo", outgate_weight, wo)
-    load("wd", decay_weight.at[pl.ds(block_start, block)], wd)
-    load("ww", write_weight.at[pl.ds(block_start, block)], ww)
+    load("wd", decay_weight.at[:, pl.ds(block_start, block)], wd)
+    load("ww", write_weight.at[:, pl.ds(block_start, block)], ww)
     load("rate", decay_rate, rate)
     load("ngain", norm_gain, ngain)
     load("st", state, st)
@@ -328,7 +332,7 @@
 
     def feed_forward(rows, gw, uw, dw, wait_down, send_buf):
         x = jnp.concatenate(rows, axis=1)
-        hidden = (silu(dot(x, gw[...])) * dot(x, uw[...])).astype(bf16)
+        hidden = (silu(dot_t(x, gw[...])) * dot_t(x, uw[...])).astype(bf16)
         wait_down()
         terms = dot(hidden, dw[...]).astype(bf16)
         for part in range(n):
@@ -345,10 +349,10 @@
     def project(x):
         parts = [dot(x, w[...]) for w in (wq, wk, wv, wo)]
         for w in (wd, ww):
-            parts.append(dot(x, w[...]))
+            parts.append(dot_t(x, w[...]))
         return parts
 
-    n_small = wd.shape[1]
+    n_small = wd.shape[0]
     spans = [i * cols for i in range(4)] + [4 * cols, 4 * cols + 128]
     lengths = [cols] * 4 + [n_small] * 2
     gains = project(jnp.broadcast_to(gain_block, (group, block)).astype(bf16))
@@ -543,6 +547,8 @@
     if args[0].shape[1] % 128 or args[17].shape[2] != 128:
         return shards_by_collectives(*args)
     args = list(args)
+    for i in (1, 2, 4, 5, 11, 12):
+        args[i] = args[i].T
     args[13] = args[13].reshape(1, -1)
     args[14] = args[14].reshape(1, -1)
     tokens, decay_weight, state = args[0], args[11], args[17]
@@ -551,7 +557,7 @@
     group, own = tokens.shape
     seqs = state.shape[0]
     block, cols = query_weight.shape
-    small = decay_weight.shape[1]
+    small = decay_weight.shape[0]
     flat = 4 * cols + 2 * 128
 
     def like(x):
@@ -560,8 +566,8 @@
     scratch = [
         pltpu.VMEM((n, group, own), bf16),
         *[like(x) for x in args[1:11]],
-        pltpu.VMEM((block, small), bf16),
-        pltpu.VMEM((block, small), bf16),
+        pltpu.VMEM((small, block), bf16),
+        pltpu.VMEM((small, block), bf16),
         *[like(x) for x in args[13:18]],
         like(state),
         like(tokens),

time: 60.5 us -> 42.8 us (0.71)
  local copies, waits for them, and re-layouts: 21.9 us -> 3.14 us
  Pallas kernels: 37.5 us -> 38.8 us
    unnamed x12 -> x2, local copies, waits for them, and re-layouts: 21.9 us -> 3.14 us
    pallas_call x1, Pallas kernels: 37.5 us -> 38.8 us  [shards(): pl.pallas_call(functools.partial(kernel, n_kv, n_tp), out_shape=(jax.Shap...]
where the time goes in v2:
time: 42.8 us; the launch traced here: 42.6 us
  Pallas kernels  38.8 us (91%)
  local copies, waits for them, and re-layouts  3.14 us (7%)
  between operations  0.65 us (2%)
    pallas_call x1, Pallas kernels, shards(): pl.pallas_call(functools.partial(kernel, n_kv, n_tp), out_shape=(jax.Shap...  38.8 us
    unnamed x2, local copies, waits for them, and re-layouts  3.14 us

profile of v2, /device:TPU:0, one launch (start us, length us, event | category | flops | bytes accessed | tf_op | source)
XLA Modules:
  0.0 42.6 jit_solution(10643734030061618861)
XLA Ops:
  0.6 38.8 %shard_map.185 = (bf16[8,256]{1,0:T(8,128)(2,1)}, f32[2,4,128,128]{3,2,1,0:T(8,128)}) custom-call(bf16[8,256]{1,0:T(8,128)(2,1)} %tokens.1, bf16[704,2048]{1,0:T(8,128)(2,1)} %bitcast.8, bf16[704,2048]{1,0:T(8,128)(2,1)} %bitcast.9, bf16[704,2048]{1,0:T(8,128)(2,1)} %down_first.1, bf16[704,2048]{1,0:T(8,128)(2,1)} %bitcast.10, bf16[704,2048]{1,0:T(8,128)(2,1)} %bitcast.11, ...), custom_call_target="tpu_custom_call" | custom-call | tf_op jit(solution)/shard_map/pallas_call | solution.py:593
  39.5 1.3 %copy.22 = bf16[8,256]{1,0:T(8,128)(2,1)} copy(bf16[8,256]{1,0:T(8,128)(2,1)} %get-tuple-element.4) | data formatting | bytes 8192
  40.8 1.9 %copy.23 = f32[2,4,128,128]{3,2,1,0:T(8,128)} copy(f32[2,4,128,128]{3,2,1,0:T(8,128)} %get-tuple-element.5) | data formatting | bytes 1048576

commit v3 on v2

--- a/solution.py
+++ b/solution.py
@@ -13,7 +13,7 @@
 f32 = jnp.float32
 bf16 = jnp.bfloat16
 
-TOK, RED1, GAINS, PAIR, STAT, PROJ, HEADS, MIX, ROWS2, RED2, STAT2 = range(11)
+TOK, RED1, GAINS, FIRST, PROJ, HEADS, MIX, RED2, STAT2 = range(9)
 
 
 def finish_norm(values, total, squares, width, gain):
@@ -209,14 +209,13 @@
     red_out2,
     red_in2,
     gain_buf,
-    pair_buf,
-    stat_buf,
+    first_buf,
     proj_out,
     proj_in,
     head_buf,
-    mix_out,
-    mix_in,
-    rows_buf,
+    mix_buf,
+    mixed_buf,
+    own_block,
     stat2_buf,
     stat_rows,
     load_sem,
@@ -233,7 +232,6 @@
     seqs, heads, dk, dv = state.shape
     pairs = seqs * heads
     cols = heads * dk
-    own_start = pl.multiple_of(me * own, own)
     block_start = pl.multiple_of(kv * block, block)
 
     loads = {}
@@ -261,12 +259,18 @@
     load("u2", up_second, u2)
     load("d2", down_second, d2)
 
+    ring = sorted(range(n_kv), key=lambda d: min(d, n_kv - d))
+    near = [(dk, dt) for dk in ring for dt in range(n_tp)]
+    partners = [p for p in near if p[0] == 0 and p[1]]
+    far = [p for p in near if p[0]][::-1]
+
     def peer_of(step):
-        other = lax.rem(me + step, n)
-        return other, lax.div(other, n_tp), lax.rem(other, n_tp)
+        pk = lax.rem(kv + step[0], n_kv)
+        pt = lax.rem(tp + step[1], n_tp)
+        return pk * n_tp + pt, pk, pt
 
     barrier = pltpu.get_barrier_semaphore()
-    for step in range(1, n):
+    for step in far + partners:
         _, pk, pt = peer_of(step)
         pl.semaphore_signal(
             barrier,
@@ -303,17 +307,17 @@
         ).wait_recv()
 
     def send_all(kind, src_of, dst):
-        for step in range(1, n):
+        for step in partners + far:
             other, pk, pt = peer_of(step)
             send(kind, src_of(other), dst, pk, pt)
 
     def receive_all(kind, buf):
-        for step in range(1, n):
+        for step in near[1:]:
             other, pk, pt = peer_of(step)
             receive(kind, buf.at[other], pk, pt)
 
     def send_kv(kind, src_of, dst):
-        for step in range(1, n_kv):
+        for step in ring[:0:-1]:
             pk = lax.rem(kv + step, n_kv)
             send(kind, src_of(pk), dst, pk, tp)
 
@@ -328,19 +332,27 @@
     send_all(TOK, lambda other: tok.at[me], tok.at[me])
     loads["g1"].wait()
     loads["u1"].wait()
-    receive_all(TOK, tok)
-
-    def feed_forward(rows, gw, uw, dw, wait_down, send_buf):
-        x = jnp.concatenate(rows, axis=1)
-        hidden = (silu(dot_t(x, gw[...])) * dot_t(x, uw[...])).astype(bf16)
-        wait_down()
-        terms = dot(hidden, dw[...]).astype(bf16)
-        for part in range(n):
-            send_buf[part] = terms[:, part * own : (part + 1) * own]
-
-    feed_forward([tok[s] for s in range(n)], g1, u1, d1, loads["d1"].wait, red_out)
-    send_all(RED1, lambda other: red_out.at[other], red_in.at[me])
-    red_in[me] = red_out[me]
+
+    def slot(other):
+        return pl.ds(pl.multiple_of(other * own, own), own)
+
+    def send_shares(kind, hidden, dw, send_buf, recv_buf):
+        for step in far + partners:
+            other, pk, pt = peer_of(step)
+            send_buf[other] = dot(hidden, dw[:, slot(other)]).astype(bf16)
+            send(kind, send_buf.at[other], recv_buf.at[me], pk, pt)
+        recv_buf[me] = dot(hidden, dw[:, slot(me)]).astype(bf16)
+
+    gate, up = 0.0, 0.0
+    for step in near:
+        other, pk, pt = peer_of(step)
+        if step != (0, 0):
+            receive(TOK, tok.at[other], pk, pt)
+        gate = gate + dot_t(tok[other], g1[:, slot(other)])
+        up = up + dot_t(tok[other], u1[:, slot(other)])
+    hidden = (silu(gate) * up).astype(bf16)
+    loads["d1"].wait()
+    send_shares(RED1, hidden, d1, red_out, red_in)
 
     for name in ("lgain", "wq", "wk", "wv", "wo", "wd", "ww"):
         loads[name].wait()
@@ -366,20 +378,14 @@
     for s in range(1, n):
         branch = branch + red_in[s].astype(f32)
     first = (residual_scale * tok[me].astype(f32) + 0.5 * branch).astype(bf16)
-    pair_buf[tp] = first
-    send(PAIR, pair_buf.at[tp], pair_buf.at[tp], kv, other_tp)
-    first = first.astype(f32)
-
-    def sums(values):
-        lane = lax.broadcasted_iota(jnp.int32, (group, 128), 1)
-        total = jnp.sum(values, -1, keepdims=True)
-        squares = jnp.sum(values * values, -1, keepdims=True)
-        return jnp.where(lane == 0, total, jnp.where(lane == 1, squares, 0.0))
-
-    stat_buf[me] = sums(first)
-    send_all(STAT, lambda other: stat_buf.at[me], stat_buf.at[me])
-    receive(PAIR, pair_buf.at[other_tp], kv, other_tp)
-    rows = jnp.concatenate([pair_buf[t].astype(f32) for t in range(n_tp)], axis=1)
+    first_buf[me] = first
+    send_all(FIRST, lambda other: first_buf.at[me], first_buf.at[me])
+    for step in partners:
+        other, pk, pt = peer_of(step)
+        receive(FIRST, first_buf.at[other], pk, pt)
+    rows = jnp.concatenate(
+        [first_buf[kv * n_tp + t].astype(f32) for t in range(n_tp)], axis=1
+    )
     centre = jnp.sum(rows, -1, keepdims=True) / block
     partial = project(((rows - centre) * gain_block).astype(bf16))
     for j in range(n_kv):
@@ -391,27 +397,29 @@
     send_kv(PROJ, lambda pk: proj_out.at[pk], proj_in.at[kv])
     proj_in[kv] = proj_out[kv]
 
-    receive_all(STAT, stat_buf)
+    for step in near[n_tp:]:
+        other, pk, pt = peer_of(step)
+        receive(FIRST, first_buf.at[other], pk, pt)
     receive_kv(GAINS, gain_buf)
 
-    def moments(buf):
-        total = buf[0]
-        for s in range(1, n):
-            total = total + buf[s]
-        mean = total[:, 0:1] / width
-        spread = total[:, 1:2] / width - mean * mean
-        return mean, lax.rsqrt(spread + ln_eps)
-
-    mean, rstd = moments(stat_buf)
-    own_gain = lgain[0:1, pl.ds(own_start, own)]
-    mixed_own = ((first - mean) * rstd * own_gain).astype(bf16).astype(f32)
+    def sums(values):
+        total = jnp.sum(values, -1, keepdims=True)
+        squares = jnp.sum(values * values, -1, keepdims=True)
+        return jnp.where(lane == 0, total, jnp.where(lane == 1, squares, 0.0))
+
+    def moments(total, squares):
+        mean = total / width
+        return mean, lax.rsqrt(squares / width - mean * mean + ln_eps)
+
+    values = [first_buf[s].astype(f32) for s in range(n)]
+    totals = [jnp.sum(v, -1, keepdims=True) for v in values]
+    squares = sum(jnp.sum(v * v, -1, keepdims=True) for v in values)
+    mean, rstd = moments(sum(totals), squares)
     lane = lax.broadcasted_iota(jnp.int32, (group, 128), 1)
     packed = jnp.where(lane == n_kv, rstd, 0.0)
     for j in range(n_kv):
-        local = stat_buf[j * n_tp]
-        for t in range(1, n_tp):
-            local = local + stat_buf[j * n_tp + t]
-        packed = jnp.where(lane == j, local[:, 0:1] / block - mean, packed)
+        local = sum(totals[j * n_tp : (j + 1) * n_tp])
+        packed = jnp.where(lane == j, local / block - mean, packed)
     stat_rows[...] = packed
     mine = stat_rows[pl.ds(kv * seqs, seqs), :]
 
@@ -489,42 +497,54 @@
     send_kv(HEADS, lambda pk: head_buf.at[kv], head_buf.at[kv])
     store = pltpu.make_async_copy(ns, new_state, load_sem.at[len(loads)])
     store.start()
+    for s in range(n):
+        scaled = (values[s] - mean) * rstd * lgain[0:1, s * own : (s + 1) * own]
+        mixed_buf[s] = scaled.astype(bf16)
     loads["ow"].wait()
     receive_kv(HEADS, head_buf)
     everyone = jnp.concatenate([head_buf[j].astype(f32) for j in range(n_kv)], axis=0)
-    terms = dot(everyone.astype(bf16), ow[...]).astype(bf16)
-    for t in range(n_tp):
-        mix_out[t] = terms[:, t * own : (t + 1) * own]
-    send(MIX, mix_out.at[other_tp], mix_in, kv, other_tp)
-    kept_half = mix_out[tp].astype(f32)
-    receive(MIX, mix_in, kv, other_tp)
-    mix = (kept_half + mix_in[...].astype(f32)).astype(bf16).astype(f32)
-    rows_buf[me] = (residual_scale * mixed_own + mix).astype(bf16)
-    send_all(ROWS2, lambda other: rows_buf.at[me], rows_buf.at[me])
+    mix_buf[me] = dot(everyone.astype(bf16), ow[...]).astype(bf16)
+    send_all(MIX, lambda other: mix_buf.at[me], mix_buf.at[me])
     loads["g2"].wait()
     loads["u2"].wait()
-    receive_all(ROWS2, rows_buf)
-
-    second = [rows_buf[s].astype(f32) for s in range(n)]
-    total = sum(jnp.sum(v, -1, keepdims=True) for v in second)
-    squares = sum(jnp.sum(v * v, -1, keepdims=True) for v in second)
-    mean = total / width
-    rstd = lax.rsqrt(squares / width - mean * mean + ln_eps)
-
-    def normalise(v, start):
-        return ((v - mean) * rstd * lgain[1:2, pl.ds(start, own)]).astype(bf16)
-
-    mlp_own = normalise(rows_buf[me].astype(f32), own_start).astype(f32)
-    feed_forward(
-        [normalise(v, s * own) for s, v in enumerate(second)],
-        g2,
-        u2,
-        d2,
-        loads["d2"].wait,
-        red_out2,
-    )
-    send_all(RED2, lambda other: red_out2.at[other], red_in2.at[me])
-    red_in2[me] = red_out2[me]
+
+    gate, up, total, squares = 0.0, 0.0, 0.0, 0.0
+    centre = None
+    for hop in ring:
+        for dt in range(n_tp):
+            other, pk, pt = peer_of((hop, dt))
+            if (hop, dt) != (0, 0):
+                receive(MIX, mix_buf.at[other], pk, pt)
+        pk = lax.rem(kv + hop, n_kv)
+        mix = mix_buf[pk * n_tp].astype(f32)
+        for t in range(1, n_tp):
+            mix = mix + mix_buf[pk * n_tp + t].astype(f32)
+        mixed = jnp.concatenate([mixed_buf[pk * n_tp + t] for t in range(n_tp)], axis=1)
+        second = residual_scale * mixed.astype(f32) + mix.astype(bf16).astype(f32)
+        second = second.astype(bf16).astype(f32)
+        sub = jnp.sum(second, -1, keepdims=True)
+        if centre is None:
+            centre = sub / block
+            own_block[...] = second
+        total = total + sub
+        squares = squares + jnp.sum(second * second, -1, keepdims=True)
+        span = pl.ds(pl.multiple_of(pk * block, block), block)
+        gain = lgain[1:2, span]
+        x = jnp.concatenate(
+            [(second - centre) * gain, jnp.broadcast_to(gain, (group, block))], axis=0
+        ).astype(bf16)
+        gate = gate + dot_t(x, g2[:, span])
+        up = up + dot_t(x, u2[:, span])
+    mean, rstd = moments(total, squares)
+    shift = mean - centre
+    gate = rstd * (gate[:group] - shift * gate[group : group + 1])
+    up = rstd * (up[:group] - shift * up[group : group + 1])
+    hidden = (silu(gate) * up).astype(bf16)
+    loads["d2"].wait()
+    send_shares(RED2, hidden, d2, red_out2, red_in2)
+    second_own = own_block[:, slot(tp)]
+    mlp_own = (second_own - mean) * rstd * lgain[1:2, slot(me)]
+    mlp_own = mlp_own.astype(bf16).astype(f32)
     receive_all(RED2, red_in2)
     branch = red_in2[0].astype(f32)
     for s in range(1, n):
@@ -533,8 +553,11 @@
     stat2_buf[me] = sums(third)
     send_all(STAT2, lambda other: stat2_buf.at[me], stat2_buf.at[me])
     receive_all(STAT2, stat2_buf)
-    mean, rstd = moments(stat2_buf)
-    out_v[...] = ((third - mean) * rstd * lgain[2:3, pl.ds(own_start, own)]).astype(bf16)
+    total = stat2_buf[0]
+    for s in range(1, n):
+        total = total + stat2_buf[s]
+    mean, rstd = moments(total[:, 0:1], total[:, 1:2])
+    out_v[...] = ((third - mean) * rstd * lgain[2:3, slot(me)]).astype(bf16)
     final = pltpu.make_async_copy(out_v, layer_out, load_sem.at[len(loads) + 1])
     final.start()
     for copy in sends:
@@ -576,19 +599,18 @@
         pltpu.VMEM((n, group, own), bf16),
         pltpu.VMEM((n, group, own), bf16),
         pltpu.VMEM((n_kv, 1, flat), f32),
-        pltpu.VMEM((n_tp, group, own), bf16),
-        pltpu.VMEM((n, group, 128), f32),
+        pltpu.VMEM((n, group, own), bf16),
         pltpu.VMEM((n_kv, seqs, flat), bf16),
         pltpu.VMEM((n_kv, seqs, flat), bf16),
         pltpu.VMEM((n_kv, seqs, cols), bf16),
-        pltpu.VMEM((n_tp, group, own), bf16),
-        pltpu.VMEM((group, own), bf16),
+        pltpu.VMEM((n, group, n_tp * own), bf16),
         pltpu.VMEM((n, group, own), bf16),
+        pltpu.VMEM((group, n_tp * own), f32),
         pltpu.VMEM((n, group, 128), f32),
         pltpu.VMEM((group, 128), f32),
         pltpu.SemaphoreType.DMA((20,)),
-        pltpu.SemaphoreType.DMA((11, n)),
-        pltpu.SemaphoreType.DMA((11, n)),
+        pltpu.SemaphoreType.DMA((9, n)),
+        pltpu.SemaphoreType.DMA((9, n)),
     ]
     return pl.pallas_call(
         functools.partial(kernel, n_kv, n_tp),

time: 42.8 us -> 42.4 us (level)
    pallas_call x1, Pallas kernels: 38.8 us -> 38.4 us  [shards(): pl.pallas_call(functools.partial(kernel, n_kv, n_tp), out_shape=(jax.Shap...]
where the time goes in v3:
time: 42.4 us; the launch traced here: 42.2 us
  Pallas kernels  38.4 us (91%)
  local copies, waits for them, and re-layouts  3.14 us (7%)
  between operations  0.65 us (2%)
    pallas_call x1, Pallas kernels, shards(): pl.pallas_call(functools.partial(kernel, n_kv, n_tp), out_shape=(jax.Shap...  38.4 us
    unnamed x2, local copies, waits for them, and re-layouts  3.14 us

profile of v3, /device:TPU:0, one launch (start us, length us, event | category | flops | bytes accessed | tf_op | source)
XLA Modules:
  0.0 42.2 jit_solution(16122035043119667726)
XLA Ops:
  0.6 38.4 %shard_map.185 = (bf16[8,256]{1,0:T(8,128)(2,1)}, f32[2,4,128,128]{3,2,1,0:T(8,128)}) custom-call(bf16[8,256]{1,0:T(8,128)(2,1)} %tokens.1, bf16[704,2048]{1,0:T(8,128)(2,1)} %bitcast.8, bf16[704,2048]{1,0:T(8,128)(2,1)} %bitcast.9, bf16[704,2048]{1,0:T(8,128)(2,1)} %down_first.1, bf16[704,2048]{1,0:T(8,128)(2,1)} %bitcast.10, bf16[704,2048]{1,0:T(8,128)(2,1)} %bitcast.11, ...), custom_call_target="tpu_custom_call" | custom-call | tf_op jit(solution)/shard_map/pallas_call | solution.py:615
  39.1 1.3 %copy.22 = bf16[8,256]{1,0:T(8,128)(2,1)} copy(bf16[8,256]{1,0:T(8,128)(2,1)} %get-tuple-element.4) | data formatting | bytes 8192
  40.3 1.9 %copy.23 = f32[2,4,128,128]{3,2,1,0:T(8,128)} copy(f32[2,4,128,128]{3,2,1,0:T(8,128)} %get-tuple-element.5) | data formatting | bytes 1048576

commit v4 on v3

--- a/solution.py
+++ b/solution.py
@@ -612,6 +612,7 @@
         pltpu.SemaphoreType.DMA((9, n)),
         pltpu.SemaphoreType.DMA((9, n)),
     ]
+    args = [pltpu.with_memory_space_constraint(a, pltpu.HBM) for a in args]
     return pl.pallas_call(
         functools.partial(kernel, n_kv, n_tp),
         out_shape=(
@@ -622,7 +623,7 @@
         out_specs=(pl.BlockSpec(memory_space=pl.ANY),) * 2,
         scratch_shapes=scratch,
         compiler_params=pltpu.CompilerParams(
-            collective_id=0, has_side_effects=True, vmem_limit_bytes=60 * 1024 * 1024
+            collective_id=0, has_side_effects=True, vmem_limit_bytes=40 * 1024 * 1024
         ),
     )(*args)
 

time: 42.4 us -> 40.1 us (0.946)
  local copies, waits for them, and re-layouts: 3.14 us -> 1.39 us
  Pallas kernels: 38.4 us -> 37.9 us
    unnamed x2, local copies, waits for them, and re-layouts: 3.14 us -> 1.39 us
    pallas_call x1, Pallas kernels: 38.4 us -> 37.9 us  [shards(): pl.pallas_call(functools.partial(kernel, n_kv, n_tp), out_shape=(jax.Shap...]
where the time goes in v4:
time: 40.1 us; the launch traced here: 40 us
  Pallas kernels  37.9 us (95%)
  local copies, waits for them, and re-layouts  1.39 us (3%)
  between operations  0.65 us (2%)
    pallas_call x1, Pallas kernels, shards(): pl.pallas_call(functools.partial(kernel, n_kv, n_tp), out_shape=(jax.Shap...  37.9 us
    unnamed x2, local copies, waits for them, and re-layouts  1.39 us

profile of v4, /device:TPU:0, one launch (start us, length us, event | category | flops | bytes accessed | tf_op | source)
XLA Modules:
  0.0 40.0 jit_solution(13048569674394503539)
XLA Ops:
  0.6 37.9 %shard_map.185 = (bf16[8,256]{1,0:T(8,128)(2,1)S(1)}, f32[2,4,128,128]{3,2,1,0:T(8,128)S(1)}) custom-call(bf16[8,256]{1,0:T(8,128)(2,1)} %tokens.1, bf16[704,2048]{1,0:T(8,128)(2,1)} %bitcast.8, bf16[704,2048]{1,0:T(8,128)(2,1)} %bitcast.9, bf16[704,2048]{1,0:T(8,128)(2,1)} %down_first.1, bf16[704,2048]{1,0:T(8,128)(2,1)} %bitcast.10, ...), custom_call_target="tpu_custom_call" | custom-call | tf_op jit(solution)/shard_map/pallas_call | solution.py:616
  38.6 0.6 %copy.22 = bf16[8,256]{1,0:T(8,128)(2,1)} copy(bf16[8,256]{1,0:T(8,128)(2,1)S(1)} %get-tuple-element.4) | data formatting | bytes 8192
  39.2 0.8 %copy.23 = f32[2,4,128,128]{3,2,1,0:T(8,128)} copy(f32[2,4,128,128]{3,2,1,0:T(8,128)S(1)} %get-tuple-element.5) | data formatting | bytes 1048576
